TPU v7x, 512 devices: a whole 4x4x16 slice. The times are simulated.
512 devices in a mesh: sp: 16 (over z), fs: 4 (over y), tp: 8 (over x, core).
Axes of the slice: x: 4, y: 4, z: 16, core: 2. Of those that a mesh axis runs over, the one named last changes fastest.
Arguments:
- activations: bfloat16 [8192, 4096], P(('fs', 'sp'), 'tp'), parts along dimension 0, may hold values from -6 to 6
- input_norm_gain: float32 [4096], replicated, may hold values from 0.1 to 1.9
- window_query_weight: bfloat16 [4096, 2048], P('sp', 'tp'), may hold values from -0.09375 to 0.09375
- window_key_weight: bfloat16 [4096, 512], P('sp', 'tp'), may hold values from -0.09375 to 0.09375
- window_value_weight: bfloat16 [4096, 512], P('sp', 'tp'), may hold values from -0.09375 to 0.09375
- linear_query_weight: bfloat16 [4096, 1024], P('sp', 'tp'), may hold values from -0.09375 to 0.09375
- linear_key_weight: bfloat16 [4096, 1024], P('sp', 'tp'), may hold values from -0.09375 to 0.09375
- linear_value_weight: bfloat16 [4096, 2048], P('sp', 'tp'), may hold values from -0.09375 to 0.09375
- decay_down_factor: bfloat16 [4096, 16], replicated, may hold values from -0.09375 to 0.09375
- decay_up_factor: bfloat16 [16, 1024], P(None, 'tp'), may hold values from -1.5 to 1.5
- decay_offset_bias: float32 [1024], P('tp'), may hold values from -0.5 to 9
- extra_fading_exponent: float32 [8192, 8], P(('fs', 'sp'), 'tp'), parts along dimension 0, may hold values from -1.5 to 0
- starting_state: float32 [8, 128, 256], P('tp'), may hold values from -12 to 12
- head_sink_logit: float32 [32], P('tp'), may hold values from 1 to 5
- linear_head_gain: float32 [256], replicated, may hold values from 0.1 to 1.9
- window_output_weight: bfloat16 [2048, 4096], P('tp', 'sp'), may hold values from -0.09375 to 0.09375
- linear_output_weight: bfloat16 [2048, 4096], P('tp', 'sp'), may hold values from -0.09375 to 0.09375
Outputs:
- mixer_output: bfloat16 [8192, 4096], P(('fs', 'sp', 'tp')), parts along dimension 0
There are 4 independent parts, one for each index of `fs`. A program takes and returns all parts, laid end to end along the dimension named above; an argument that names none is the same for every part. Nothing has to cross between parts.
All inputs are finite; a program needn't handle non-finite values.
Results may differ from a plain program's by a relative error of at most 0.019.
Values may be sent and summed in bfloat16 or wider, within the bound.
A program may use at most 64 MiB of HBM per device.

v0:
```python
import jax
import jax.numpy as jnp
from jax import lax
from jax.sharding import PartitionSpec as P

QH = 32
HD = 64
WINDOW = 128
LOOKUP_FEATURES = 128
DV = 256
SPAN = 64


EPS = 1e-05
FADING_SOFTNESS = 16.0
HIGH_PRECISION = lax.Precision.HIGHEST


def passed_along(value, axis, steps):
    count = lax.axis_size(axis)
    leading, last = (max(0, -steps), min(count, count - steps))
    return lax.ppermute(value, axis, [(source, source + steps) for source in range(leading, last)])


def from_everyone(x, axis):
    peers = lax.axis_size(axis)
    return lax.all_to_all(jnp.broadcast_to(x[None], (peers, *x.shape)), axis, 0, 0, tiled=True)


def folded_in_pairs(pieces, combine):
    while len(jax.tree.leaves(pieces)[0]) > 1:
        pieces = jax.vmap(combine)(
            *(jax.tree.map(lambda part: part[side::2], pieces) for side in (0, 1))
        )
    return jax.tree.map(lambda part: part[0], pieces)


def entering(x, axis, combine, identity):
    peers, place = (lax.axis_size(axis), lax.axis_index(axis))
    passed = jnp.arange(peers) < place

    def kept(part, zero, own):
        part = jnp.where(
            passed.reshape(-1, *(1 for _ in own.shape)),
            part.astype(own.dtype),
            jnp.asarray(zero, own.dtype),
        )
        return part

    pieces = jax.tree.map(
        lambda part: from_everyone(part, axis),
        jax.tree.map(lambda part, kind: part.astype(kind), x, (jnp.bfloat16, jnp.bfloat16)),
    )
    return folded_in_pairs(jax.tree.map(kept, pieces, identity, x), combine)


def joined_along(pieces, dim):
    lengths = list(pieces.shape[1:])
    lengths[dim] *= pieces.shape[0]
    return jnp.moveaxis(pieces, 0, dim).reshape(lengths)


def gather_directly(x, axis, dim):
    pieces = from_everyone(x, axis)
    return joined_along(pieces, dim)


def in_one_piece(arrays, axis, dim, along):
    both = jnp.concatenate(arrays, axis=along)
    whole, at, gathered = (lax.all_gather(both, axis, axis=dim, tiled=True), 0, [])
    for a in arrays:
        gathered.append(lax.slice_in_dim(whole, at, at + a.shape[along], axis=along))
        at += a.shape[along]
    return tuple(gathered)


def cut_along(x, dim, peers):
    lengths = x.shape
    pieces = x.reshape(*lengths[:dim], peers, lengths[dim] // peers, *lengths[dim + 1 :])
    return jnp.moveaxis(pieces, dim, 0)


def summed_on_arrival(x, axis, dim):
    pieces = cut_along(x, dim, lax.axis_size(axis))
    arrived = lax.all_to_all(pieces, axis, split_axis=0, concat_axis=0, tiled=True)
    return arrived.astype(jnp.float32).sum(axis=0)


def window_attention(near_query, near_keys, near_values, head_sink_logit):
    stream_extent = near_query.shape[0]
    key_heads = near_keys.shape[1] // HD
    heads_here = near_query.shape[1] // HD
    groups = heads_here // key_heads
    blocks = stream_extent // WINDOW
    tail_rows = jnp.stack([near_keys, near_values])
    before = passed_along(tail_rows, "sp", 1)

    def banded(previous, current):
        extended = jnp.concatenate([previous, current], axis=0)
        earlier = extended[:stream_extent].reshape(blocks, WINDOW, key_heads, HD)
        present = extended[WINDOW:].reshape(blocks, WINDOW, key_heads, HD)
        return jnp.concatenate([earlier, present], axis=1)

    key_band = banded(before[0], near_keys)
    value_band = banded(before[1], near_values)
    queries = near_query.reshape(blocks, WINDOW, key_heads, groups, HD)
    scores = jnp.einsum(
        "nqhgd,nkhd->hgnqk", queries, key_band, preferred_element_type=jnp.float32
    ) * HD ** (-0.5)
    head_ids = lax.axis_index("tp") * heads_here + jnp.arange(heads_here, dtype=jnp.int32)
    slopes = jnp.exp2(-8.0 * (head_ids + 1).astype(jnp.float32) / QH).reshape(key_heads, groups)
    query_pos = jnp.arange(WINDOW, dtype=jnp.int32)
    key_pos = jnp.arange(2 * WINDOW, dtype=jnp.int32)
    distance = query_pos[:, None] - key_pos[None, :] + WINDOW
    start_pos = (
        lax.axis_index("sp") * stream_extent + (jnp.arange(blocks, dtype=jnp.int32) - 1) * WINDOW
    )
    absolute = start_pos[:, None] + key_pos[None, :]
    allowed = ((distance >= 0) & (distance < WINDOW))[None] & (absolute >= 0)[:, None, :]
    biased = scores - slopes[:, :, None, None, None] * distance.astype(jnp.float32)
    weights = jnp.where(allowed, jnp.exp(biased), 0.0)
    denominator = (
        jnp.sum(weights, axis=-1, keepdims=True)
        + jnp.exp(head_sink_logit.reshape(key_heads, groups))[:, :, None, None, None]
    )
    attention = (weights / denominator).astype(jnp.bfloat16)
    attended = jnp.einsum(
        "hgnqk,nkhd->nqhgd", attention, value_band, preferred_element_type=jnp.float32
    )
    return attended.reshape(stream_extent, heads_here * HD).astype(jnp.bfloat16)


def linear_attention(
    gated_query, gated_keys, gated_values, fading_exponent, linear_head_gain, starting_state
):
    stream_extent = gated_query.shape[0]
    head_total = gated_query.shape[1] // LOOKUP_FEATURES
    span_count = stream_extent // SPAN
    scaled_query = gated_query.astype(jnp.float32).reshape(
        span_count, SPAN, head_total, LOOKUP_FEATURES
    ) * LOOKUP_FEATURES ** (-0.5)
    keys_wide = gated_keys.astype(jnp.float32).reshape(
        span_count, SPAN, head_total, LOOKUP_FEATURES
    )
    values_wide = gated_values.astype(jnp.float32).reshape(span_count, SPAN, head_total, DV)
    running = jnp.cumsum(
        fading_exponent.reshape(span_count, SPAN, head_total, LOOKUP_FEATURES), axis=1
    )
    span_end = running[:, -1]
    query_with_decay = scaled_query * jnp.exp(running)
    inverse_keys = keys_wide * jnp.exp(-running)
    ending_keys = keys_wide * jnp.exp(span_end[:, None] - running)
    inner = jnp.einsum("nchk,nshk->nhcs", query_with_decay, inverse_keys, precision=HIGH_PRECISION)
    lower = jnp.tril(jnp.ones((SPAN, SPAN), dtype=bool))
    inner = jnp.where(lower, inner, 0.0)
    within = jnp.einsum("nhcs,nshv->nchv", inner, values_wide, precision=HIGH_PRECISION)

    def advance(running_state, inputs):
        query_portion, key_portion, value_portion, scale_factor = inputs
        layer_output = jnp.einsum(
            "fmy,mys->fms", query_portion, running_state, precision=HIGH_PRECISION
        )
        running_state = running_state * scale_factor[..., None] + jnp.einsum(
            "gxp,gxz->xpz", key_portion, value_portion, precision=HIGH_PRECISION
        )
        return (running_state, layer_output)

    start_state = jnp.zeros((head_total, LOOKUP_FEATURES, DV), jnp.float32)
    state_end, carried = lax.scan(
        advance, start_state, (query_with_decay, ending_keys, values_wide, jnp.exp(span_end))
    )
    device_decay = jnp.exp(jnp.sum(span_end, axis=0))
    prefix_sums = jnp.cumsum(span_end, axis=0) - span_end

    def combine(earlier, later):
        return (earlier[0] * later[0], later[0][..., None] * earlier[1] + later[1])

    decay_before, state_before = entering(
        (device_decay, state_end),
        "sp",
        combine,
        (jnp.ones_like(device_decay), jnp.zeros_like(state_end)),
    )
    incoming_rows = state_before + decay_before[..., None] * starting_state
    crossing = jnp.einsum(
        "qwso,soz->qwsz",
        query_with_decay * jnp.exp(prefix_sums)[:, None],
        incoming_rows,
        precision=HIGH_PRECISION,
    )
    flat = (within + carried + crossing).reshape(stream_extent, head_total, DV)
    normal = (
        flat * lax.rsqrt(jnp.mean(flat * flat, axis=-1, keepdims=True) + EPS) * linear_head_gain
    )
    return normal.reshape(stream_extent, head_total * DV).astype(jnp.bfloat16)


def local(
    activations,
    input_norm_gain,
    window_query_weight,
    window_key_weight,
    window_value_weight,
    linear_query_weight,
    linear_key_weight,
    linear_value_weight,
    decay_down_factor,
    decay_up_factor,
    decay_offset_bias,
    extra_fading_exponent,
    starting_state,
    head_sink_logit,
    linear_head_gain,
    window_output_weight,
    linear_output_weight,
):
    gathered = gather_directly(activations, "tp", 1)
    widened = gathered.astype(jnp.float32)
    normed = (
        widened
        * lax.rsqrt(jnp.mean(widened * widened, axis=1, keepdims=True) + EPS)
        * input_norm_gain
    ).astype(jnp.bfloat16)
    row_total = normed.shape[0]
    matrices = (
        window_query_weight,
        window_key_weight,
        window_value_weight,
        linear_query_weight,
        linear_key_weight,
        linear_value_weight,
    )
    segments = in_one_piece(
        (matrices[0], matrices[1], matrices[2], matrices[3], matrices[4], matrices[5]), "sp", 0, 1
    )
    projected = tuple(
        (jnp.dot(normed, segment, preferred_element_type=jnp.float32) for segment in segments)
    )
    near_query, near_keys, near_values, gated_query, gated_keys, gated_values = [
        product.astype(jnp.bfloat16) for product in projected
    ]
    low_rank = jnp.dot(normed, decay_down_factor, preferred_element_type=jnp.float32).astype(
        jnp.bfloat16
    )
    attention_energies = (
        jnp.dot(low_rank, decay_up_factor, preferred_element_type=jnp.float32) + decay_offset_bias
    )
    head_total = extra_fading_exponent.shape[1]
    fading_exponent = (jax.nn.log_sigmoid(attention_energies) / FADING_SOFTNESS).reshape(
        row_total, head_total, LOOKUP_FEATURES
    ) + extra_fading_exponent[:, :, None]
    near_out = window_attention(near_query, near_keys, near_values, head_sink_logit)
    gated_out = linear_attention(
        gated_query, gated_keys, gated_values, fading_exponent, linear_head_gain, starting_state
    )
    window_full, linear_full = in_one_piece(
        (window_output_weight, linear_output_weight), "sp", 1, 0
    )
    summed = summed_on_arrival(
        (
            jnp.dot(near_out, window_full, preferred_element_type=jnp.float32)
            + jnp.dot(gated_out, linear_full, preferred_element_type=jnp.float32)
        ).astype(jnp.bfloat16),
        "tp",
        0,
    )
    return summed.astype(jnp.bfloat16)


def solution(mesh):
    placed = (
        P(("fs", "sp"), "tp"),
        P(),
        P("sp", "tp"),
        P("sp", "tp"),
        P("sp", "tp"),
        P("sp", "tp"),
        P("sp", "tp"),
        P("sp", "tp"),
        P(),
        P(None, "tp"),
        P("tp"),
        P(("fs", "sp"), "tp"),
        P("tp", None, None),
        P("tp"),
        P(),
        P("tp", "sp"),
        P("tp", "sp"),
    )
    return jax.shard_map(
        local, mesh=mesh, in_specs=placed, out_specs=P(("fs", "sp", "tp"), None), check_vma=False
    )
```

profile of v0, /device:TPU:1, one launch (start us, length us, event | category | flops | bytes accessed | tf_op | source)
XLA Modules:
  0.0 280.5 jit_solution(3121717669468387975)
XLA Ops:
  6.5 0.9 copy.29
  7.4 0.9 copy.30
  8.3 1.9 concatenate.12
  10.3 1.1 copy.28
  11.4 1.1 broadcast_in_dim.53
  12.5 10.4 %all-to-all-start = ((bf16[8,128,512]{1,2,0:T(8,128)(2,1)}), bf16[8,128,512]{1,2,0:T(8,128)(2,1)S(1)}, u32[]{:S(2)}, u32[]{:S(2)}) async-start(bf16[8,128,512]{1,2,0:T(8,128)(2,1)} %broadcast_in_dim.53), calls=%async_computation | async-start | bytes 2097152 | tf_op jit(solution)/shard_map/all_to_all | solution.py:27
  24.0 13.9 %all-to-all-done = bf16[8,128,512]{1,2,0:T(8,128)(2,1)S(1)} async-done(((bf16[8,128,512]{1,2,0:T(8,128)(2,1)}), bf16[8,128,512]{1,2,0:T(8,128)(2,1)S(1)}, u32[]{:S(2)}, u32[]{:S(2)}) %all-to-all-start) | async-done | bytes 1048608 | tf_op jit(solution)/shard_map/all_to_all | solution.py:27
  40.6 10.4 %all-to-all-start.1 = ((bf16[16,1,128]{2,1,0:T(2,128)(2,1)}), bf16[16,1,128]{2,1,0:T(2,128)(2,1)S(1)}, u32[]{:S(2)}, u32[]{:S(2)}) async-start(bf16[16,1,128]{2,1,0:T(2,128)(2,1)} %broadcast_in_dim.64), calls=%async_computation.1 | async-start | bytes 16384 | tf_op jit(solution)/shard_map/all_to_all | solution.py:27
  51.0 60.3 %all-gather.3.cloned.1.call-done = bf16[4096,896]{1,0:T(8,128)(2,1)} async-done(((bf16[256,896]{1,0:T(8,128)(2,1)}), bf16[4096,896]{1,0:T(8,128)(2,1)}) %all-gather.3.cloned.1.call-update) | async-done | bytes 7340048 | tf_op jit(solution)/shard_map/all_gather | solution.py:70
  111.3 2.2 fusion.30
  113.5 1.7 fusion.36
  115.2 1.7 fusion.34
  117.1 1.3 while.13
  118.5 1.1 broadcast_in_dim.103
  119.6 8.6 %all-to-all-start.2 = ((bf16[16,1,128,256]{3,2,1,0:T(8,128)(2,1)}), bf16[16,1,128,256]{3,2,1,0:T(8,128)(2,1)S(1)}, u32[]{:S(2)}, u32[]{:S(2)}) async-start(bf16[16,1,128,256]{3,2,1,0:T(8,128)(2,1)} %broadcast_in_dim.103), calls=%async_computation.2 | async-start | bytes 2097152 | tf_op jit(solution)/shard_map/all_to_all | solution.py:27
  128.8 1.7 convolution_convert_fusion.5
  130.6 2.2 convolution_convert_fusion.4
  132.8 3.3 %collective-permute-start = (bf16[2,128,64]{1,2,0:T(8,128)(2,1)S(1)}, bf16[2,128,64]{1,2,0:T(8,128)(2,1)S(1)}, u32[]{:S(2)}, u32[]{:S(2)}) collective-permute-start(bf16[2,128,64]{1,2,0:T(8,128)(2,1)S(1)} %pad_maximum_fusion.1), channel_id=1, source_target_pairs={{0,32},{32,64},{64,96},{96,128},{128,160},{160,192},{192,224},{224... | collective-permute-start | bytes 98312 | tf_op jit(solution)/shard_map/ppermute | solution.py:22
  136.3 2.2 fusion.27
  138.9 30.8 %collective-permute-done = bf16[2,128,64]{1,2,0:T(8,128)(2,1)S(1)} collective-permute-done((bf16[2,128,64]{1,2,0:T(8,128)(2,1)S(1)}, bf16[2,128,64]{1,2,0:T(8,128)(2,1)S(1)}, u32[]{:S(2)}, u32[]{:S(2)}) %collective-permute-start) | collective-permute-done | bytes 32800 | tf_op jit(solution)/shard_map/ppermute | solution.py:22
  170.2 65.9 %all-gather.5.cloned.1.call-done = bf16[512,4096]{1,0:T(8,128)(2,1)} async-done(((bf16[512,256]{1,0:T(8,128)(2,1)}), bf16[512,4096]{1,0:T(8,128)(2,1)}) %all-gather.5.cloned.1.call-update) | async-done | bytes 4194320 | tf_op jit(solution)/shard_map/all_gather | solution.py:70
  236.1 2.1 fusion.15
  240.6 2.0 fusion.11
  242.7 30.2 %all_to_all.20 = bf16[8,16,4096]{2,1,0:T(8,128)(2,1)S(1)} all-to-all(bf16[8,16,4096]{2,1,0:T(8,128)(2,1)S(1)} %bitcast.182), channel_id=1, replica_groups=mesh['sp'=16,'fs'=4,'tp'=8] {'tp'}, dimensions={0} | all-to-all | bytes 2097152 | tf_op jit(solution)/shard_map/all_to_all | solution.py:85
  (83 shorter events, 10.0 us)
Async XLA Ops:
  6.5 32.7 %copy-start = (bf16[4096,16]{0,1:T(8,128)(2,1)S(1)}, bf16[4096,16]{0,1:T(8,128)(2,1)}, u32[]{:S(2)}) copy-start(bf16[4096,16]{0,1:T(8,128)(2,1)} %param.27) | copy-start | bytes 393220
  6.5 104.7 %all-gather.3.cloned.1.call-start = ((), (), s32[]{:S(2)}) async-start(), calls=%async_computation.4 | async-start | bytes 7798784 | tf_op jit(solution)/shard_map/all_gather | solution.py:70
  10.3 12.7 %copy-start.1 = (bf16[256,256]{1,0:T(8,128)(2,1)S(1)}, bf16[256,256]{1,0:T(8,128)(2,1)}, u32[]{:S(2)}) copy-start(bf16[256,256]{1,0:T(8,128)(2,1)} %param.35) | copy-start | bytes 393220
  10.3 12.7 %copy-start.2 = (bf16[256,256]{1,0:T(8,128)(2,1)S(1)}, bf16[256,256]{1,0:T(8,128)(2,1)}, u32[]{:S(2)}) copy-start(bf16[256,256]{1,0:T(8,128)(2,1)} %param.34) | copy-start | bytes 393220
  11.4 12.4 %copy-start.9 = (f32[4]{0:T(128)S(1)}, f32[4]{0:T(128)}, u32[]{:S(2)}) copy-start(f32[4]{0:T(128)} %param.32) | copy-start | bytes 52
  12.5 26.0 %copy-start.4 = (f32[4096]{0:T(1024)S(1)}, f32[4096]{0:T(1024)}, u32[]{:S(2)}) copy-start(f32[4096]{0:T(1024)} %param.20) | copy-start | bytes 49156
  12.5 25.4 %all-to-all-start = ((bf16[8,128,512]{1,2,0:T(8,128)(2,1)}), bf16[8,128,512]{1,2,0:T(8,128)(2,1)S(1)}, u32[]{:S(2)}, u32[]{:S(2)}) async-start(bf16[8,128,512]{1,2,0:T(8,128)(2,1)} %broadcast_in_dim.53), calls=%async_computation | async-start | bytes 2097152 | tf_op jit(solution)/shard_map/all_to_all | solution.py:27
  23.0 16.3 %copy-start.8 = (bf16[16,128]{1,0:T(8,128)(2,1)S(1)}, bf16[16,128]{1,0:T(8,128)(2,1)}, u32[]{:S(2)}) copy-start(bf16[16,128]{1,0:T(8,128)(2,1)} %param.28) | copy-start | bytes 12292
  23.0 16.3 %copy-start.10 = (f32[128,1]{0,1:T(1,128)S(1)}, f32[128,1]{0,1:T(1,128)}, u32[]{:S(2)}) copy-start(f32[128,1]{0,1:T(1,128)} %param.30) | copy-start | bytes 1540
  23.0 16.3 %copy-start.11 = (f32[128]{0:T(128)S(1)}, f32[128]{0:T(128)}, u32[]{:S(2)}) copy-start(f32[128]{0:T(128)} %param.29) | copy-start | bytes 1540
  23.0 213.1 %all-gather.5.cloned.1.call-start = ((), (), s32[]{:S(2)}) async-start(), calls=%async_computation.5 | async-start | bytes 4456448 | tf_op jit(solution)/shard_map/all_gather | solution.py:70
  23.8 104.3 %copy-start.6 = (pred[16]{0:T(512)(128)(4,1)}, pred[16]{0:T(512)(128)(4,1)S(1)}, u32[]{:S(2)}) copy-start(pred[16]{0:T(512)(128)(4,1)S(1)} %iota_compare_fusion.1) | copy-start | bytes 52
  40.6 77.8 %all-to-all-start.1 = ((bf16[16,1,128]{2,1,0:T(2,128)(2,1)}), bf16[16,1,128]{2,1,0:T(2,128)(2,1)S(1)}, u32[]{:S(2)}, u32[]{:S(2)}) async-start(bf16[16,1,128]{2,1,0:T(2,128)(2,1)} %broadcast_in_dim.64), calls=%async_computation.1 | async-start | bytes 16384 | tf_op jit(solution)/shard_map/all_to_all | solution.py:27
  119.6 118.6 %all-to-all-start.2 = ((bf16[16,1,128,256]{3,2,1,0:T(8,128)(2,1)}), bf16[16,1,128,256]{3,2,1,0:T(8,128)(2,1)S(1)}, u32[]{:S(2)}, u32[]{:S(2)}) async-start(bf16[16,1,128,256]{3,2,1,0:T(8,128)(2,1)} %broadcast_in_dim.103), calls=%async_computation.2 | async-start | bytes 2097152 | tf_op jit(solution)/shard_map/all_to_all | solution.py:27
  132.8 36.8 %collective-permute-start = (bf16[2,128,64]{1,2,0:T(8,128)(2,1)S(1)}, bf16[2,128,64]{1,2,0:T(8,128)(2,1)S(1)}, u32[]{:S(2)}, u32[]{:S(2)}) collective-permute-start(bf16[2,128,64]{1,2,0:T(8,128)(2,1)S(1)} %pad_maximum_fusion.1), channel_id=1, source_target_pairs={{0,32},{32,64},{64,96},{96,128},{128,160},{160,192},{192,224},{224... | collective-permute-start | bytes 98312 | tf_op jit(solution)/shard_map/ppermute | solution.py:22
  239.0 0.9 copy-start.3
  239.1 0.9 copy-start.5
  239.3 1.2 copy-start.7
Sparse Core Ops, SparseCore 0:
  10.4 100.8 all-gather.2
  113.3 122.7 all-gather.4
where the time goes:
time: 281 us; the launch traced here: 280 us
  waiting for transfers between devices  171 us (61%)
  starting transfers between devices  32.7 us (12%)
  blocking collectives  30.2 us (11%)
  matrix products  18.9 us (7%)
  between operations  13.9 us (5%)
  local copies, waits for them, and re-layouts  8.35 us (3%)
  other arithmetic  5.48 us (2%)
    all_gather x2, waiting for transfers between devices, in_one_piece(): lax.all_gather(both, axis, axis=dim, tiled=True)  126 us
    ppermute x1, waiting for transfers between devices, passed_along(): lax.ppermute(value, axis, [(source, source + steps) for source in range(l...  30.8 us
    all_to_all x1, blocking collectives, summed_on_arrival(): lax.all_to_all(pieces, axis, split_axis=0, concat_axis=0, tiled=True)  30.2 us
    all_to_all x3, starting transfers between devices, from_everyone(): lax.all_to_all(jnp.broadcast_to(x[None], (peers, *x.shape)), axis, 0, 0,...  29.4 us
    all_to_all x3, waiting for transfers between devices, from_everyone(): lax.all_to_all(jnp.broadcast_to(x[None], (peers, *x.shape)), axis, 0, 0,...  13.9 us
    dot_general x6, matrix products, local(): jnp.dot(normed, segment, preferred_element_type=jnp.float32)  11.7 us
  transfers between devices with their start and end apart: 6, of which 4 were waited for; matrix products, arithmetic and copies ran while one was open for 8% of the time, Pallas kernels for 0%

commit v1 on v0

v1 whole, which is shorter than its diff:
```python
import functools

import jax
import jax.numpy as jnp
from jax import lax
from jax.experimental import pallas as pl
from jax.experimental.pallas import tpu as pltpu
from jax.sharding import PartitionSpec as P

MESH = pl.DeviceIdType.MESH
HD = 64
HEADS = 4
LK = 128
DV = 256
SPAN = 64
TOK = 128
FEAT = 512
ROWS = 256
RANK = 16
EPS = 1e-05
HIGH = lax.Precision.HIGHEST
F32 = jnp.float32
BF16 = jnp.bfloat16
C_LK, C_LV, C_LQ, C_WQ, C_KV, C_END = 0, 128, 384, 512, 768, 896
STREAMS = ((0, 384), (384, 512))


def over(a, b, ca, cb, precision=None):
    return lax.dot_general(
        a, b, (((ca,), (cb,)), ((), ())), preferred_element_type=F32, precision=precision
    )


def kernel(
    SP, FS, TP,
    x_ref, gain_ref, wq_ref, wkt_ref, wvt_ref, lq_ref, lk_ref, lv_ref, ddt_ref, up_ref,
    bias_ref, extra_ref, start_ref, sink_ref, lgain_ref, wow_ref, wol_ref,
    out_ref,
    xs, xg, aux, wg, wo, wcat, rs_send, rs_recv, kv, st_send, st_recv, dlog, pre_send,
    pre_recv, startt, og, po, xr_recv, fin_send, fin_recv,
    ring_s, ring_r, y_s, y_r, x_s, x_r, a_s, a_r, d_s, d_r, rs_s, rs_r, kv_s, kv_r,
    st_s, st_r, pre_s, pre_r, og_s, og_r, xr_s, xr_r, fin_s, fin_r,
):
    s, f, t = lax.axis_index("sp"), lax.axis_index("fs"), lax.axis_index("tp")
    q = ROWS // FS
    ft = FEAT // FS
    vr = DV // SP
    tr = TOK // TP
    dim = FEAT * TP
    right, left = lax.rem(s + 1, SP), lax.rem(s + SP - 1, SP)
    pending = []

    def peer(me, offset, count):
        return lax.rem(me + offset, count)

    def copy(src, dst, send_sem, recv_sem, **device):
        return pltpu.make_async_remote_copy(
            src_ref=src, dst_ref=dst, send_sem=send_sem, recv_sem=recv_sem,
            device_id=device, device_id_type=MESH,
        )

    def send(src, dst, send_sem, recv_sem, **device):
        c = copy(src, dst, send_sem, recv_sem, **device)
        c.start()
        pending.append(c)

    def arrived(dst, send_sem, recv_sem, **device):
        copy(dst, dst, send_sem, recv_sem, **device).wait_recv()

    barrier = pltpu.get_barrier_semaphore()
    pl.semaphore_signal(barrier, inc=1, device_id={"sp": right}, device_id_type=MESH)
    pl.semaphore_signal(barrier, inc=1, device_id={"sp": left}, device_id_type=MESH)
    for o in range(1, FS):
        pl.semaphore_signal(barrier, inc=1, device_id={"fs": peer(f, o, FS)}, device_id_type=MESH)
    for o in range(1, TP):
        pl.semaphore_signal(barrier, inc=1, device_id={"tp": peer(t, o, TP)}, device_id_type=MESH)

    mine = pl.ds(pl.multiple_of(s * q, q), q)
    part = pl.ds(pl.multiple_of(f * q, q), q)
    wg[mine, C_LK:C_LV] = lk_ref[part, :]
    wg[mine, C_LV:C_LQ] = lv_ref[part, :]
    wg[mine, C_LQ:C_WQ] = lq_ref[part, :]
    wg[mine, C_WQ:C_KV] = wq_ref[part, :]
    both = jnp.concatenate([wkt_ref[...], wvt_ref[...]], axis=0).astype(F32).T.astype(BF16)
    for k in range(FS):
        @pl.when(f == k)
        def _():
            wg[mine, C_KV:C_END] = both[k * q:(k + 1) * q, :]
            wo[s] = jnp.concatenate(
                [wow_ref[:, k * q:(k + 1) * q], wol_ref[:, k * q:(k + 1) * q]], axis=1
            )

    pl.semaphore_wait(barrier, 2 + (FS - 1) + (TP - 1))

    half = SP // 2

    def chunk(stream, z):
        if stream == 2:
            return wo.at[z]
        at, width = STREAMS[stream]
        return wg.at[pl.ds(pl.multiple_of(z * q, q), q), pl.ds(at, width)]

    def ring_step(stream, k):
        for d in range(2):
            to, back = (right, left) if d == 0 else (left, right)
            count = half if d == 0 else SP - 1 - half
            z = lax.rem(s + SP - k, SP) if d == 0 else lax.rem(s + k, SP)
            if 1 <= k <= count:
                arrived(chunk(stream, z), ring_s.at[stream, d, k - 1],
                        ring_r.at[stream, d, k - 1], sp=back)
            if k < count:
                send(chunk(stream, z), chunk(stream, z), ring_s.at[stream, d, k],
                     ring_r.at[stream, d, k], sp=to)

    done = [0]

    def third():
        if done[0] <= half:
            ring_step(2, done[0])
            done[0] += 1

    ring_step(0, 0)
    ring_step(1, 0)

    xf = x_ref[...].astype(F32)
    rows = FEAT // 128
    gain = jnp.concatenate(
        [gain_ref[pl.ds(t * rows + k, 1), :] for k in range(rows)], axis=1
    )
    xw = (xf * gain).astype(BF16)
    here = pl.ds(pl.multiple_of(t * ft, ft), ft)
    for k in range(FS):
        cut = jnp.concatenate(
            [xw[:, k * q:(k + 1) * q], xw[:, ROWS + k * q:ROWS + (k + 1) * q]], axis=1
        )
        xs[k] = cut

        @pl.when(f == k)
        def _():
            xg[k, :, here] = cut
    for o in range(1, FS):
        to = peer(f, o, FS)
        send(xs.at[to], xg.at[f, :, here], y_s.at[o - 1], y_r.at[o - 1], fs=to)
    dd = ddt_ref[:, pl.ds(pl.multiple_of(t * FEAT, FEAT), FEAT)]
    aux[t, :RANK, :] = over(dd, xw, 1, 1)
    aux[t, RANK:, :] = over(jnp.ones((8, FEAT), F32), xf * xf, 1, 1, HIGH)
    for o in range(1, TP):
        send(aux.at[t], aux.at[t], a_s.at[o - 1], a_r.at[o - 1], tp=peer(t, o, TP))

    ring_step(0, 1)
    ring_step(1, 1)
    for o in range(1, FS):
        came = peer(f, FS - o, FS)
        arrived(xg.at[came, :, here], y_s.at[o - 1], y_r.at[o - 1], fs=came)
    for o in range(1, TP):
        send(xg.at[:, :, here], xg.at[:, :, here], x_s.at[o - 1], x_r.at[o - 1],
             tp=peer(t, o, TP))
    startt[...] = start_ref[...].T

    for k in range(2, half + 1):
        ring_step(0, k)
        ring_step(1, k)
        if k >= half // 2:
            third()

    for o in range(1, TP):
        came = peer(t, TP - o, TP)
        arrived(aux.at[came], a_s.at[o - 1], a_r.at[o - 1], tp=came)
    sums = aux[0]
    for k in range(1, TP):
        sums = sums + aux[k]
    scale_rows = lax.rsqrt(sums[RANK:, :] / dim + EPS)
    eighth = jnp.full((8, 128), 0.125, F32)
    scale = over(scale_rows, eighth, 0, 0, HIGH)
    low = (sums[:RANK, :] * scale_rows[0:1, :]).astype(BF16)
    energies = over(low, up_ref[...], 0, 0) + bias_ref[...]
    extra = over(jnp.broadcast_to(extra_ref[...], (8, 128)), eighth, 0, 0, HIGH)
    fading = (
        jnp.minimum(energies, 0.0) - jnp.log1p(jnp.exp(-jnp.abs(energies)))
    ) / 16.0 + extra
    ri = lax.broadcasted_iota(jnp.int32, (TOK, TOK), 0)
    ci = lax.broadcasted_iota(jnp.int32, (TOK, TOK), 1)
    tri = ((ri >= ci) & ((ri < SPAN) | (ci >= SPAN))).astype(F32)
    running = over(tri, fading, 1, 0, HIGH)
    end0, end1 = running[SPAN - 1:SPAN, :], running[TOK - 1:TOK, :]
    dlog[s] = jnp.broadcast_to(end0 + end1, (8, 128))
    for o in range(1, SP):
        send(dlog.at[s], dlog.at[s], d_s.at[o - 1], d_r.at[o - 1], sp=peer(s, o, SP))
    for o in range(1, TP):
        came = peer(t, TP - o, TP)
        there = pl.ds(pl.multiple_of(came * ft, ft), ft)
        arrived(xg.at[:, :, there], x_s.at[o - 1], x_r.at[o - 1], tp=came)

    owns = []
    for stream, (at, width) in enumerate(STREAMS):
        cols = pl.ds(at, width)
        for o in list(range(1, FS)) + [0]:
            to = peer(f, o, FS)
            product = over(xg[to], wg[:, at:at + width], 1, 0)
            if o == 0:
                owns.append(product)
            else:
                rs_send[o - 1, :, at:at + width] = product.astype(BF16)
                send(rs_send.at[o - 1, :, cols], rs_recv.at[o - 1, :, cols],
                     rs_s.at[stream, o - 1], rs_r.at[stream, o - 1], fs=to)

    def reduced(stream):
        at, width = STREAMS[stream]
        total = owns[stream]
        for o in range(1, FS):
            came = peer(f, FS - o, FS)
            arrived(rs_recv.at[o - 1, :, pl.ds(at, width)], rs_s.at[stream, o - 1],
                    rs_r.at[stream, o - 1], fs=came)
            total = total + rs_recv[o - 1, :, at:at + width].astype(F32)
        wide = jnp.concatenate([scale] * (width // 128), axis=1)
        return (total * wide).astype(BF16)

    third()
    first = reduced(0)
    keys = first[:, C_LK:C_LV].astype(F32)
    values = first[:, C_LV:C_LQ].astype(F32)
    grow = jnp.exp(running)
    ends = jnp.where(ri < SPAN, end0, end1)
    ending = keys * jnp.exp(ends - running)
    state0 = over(values[:SPAN], ending[:SPAN], 0, 0, HIGH)
    state1 = state0 * jnp.exp(end1) + over(values[SPAN:], ending[SPAN:], 0, 0, HIGH)
    packed = state1.astype(BF16)
    st_send[...] = packed.reshape(SP, vr, LK)
    st_recv[s] = st_send[s]
    for o in range(1, SP):
        to = peer(s, o, SP)
        send(st_send.at[to], st_recv.at[s], st_s.at[o - 1], st_r.at[o - 1], sp=to)

    third()
    second = reduced(1)
    kv[1] = second[:, C_KV - C_LQ:]
    send(kv.at[1], kv.at[0], kv_s, kv_r, sp=right)
    inverse = keys * jnp.exp(-running)
    query = second[:, :C_WQ - C_LQ].astype(F32) * (LK ** -0.5) * grow
    raws = []
    for n in range(2):
        span = slice(n * SPAN, (n + 1) * SPAN)
        inner = over(query[span], inverse[span], 1, 1, HIGH)
        inner = jnp.where(ri[:SPAN, :SPAN] >= ci[:SPAN, :SPAN], inner, 0.0)
        raws.append(over(inner, values[span], 1, 0, HIGH))
    raws[1] = raws[1] + over(query[SPAN:], state0, 1, 1, HIGH)

    for o in range(1, SP):
        came = peer(s, SP - o, SP)
        arrived(dlog.at[came], d_s.at[o - 1], d_r.at[o - 1], sp=came)
    for o in range(1, SP):
        came = peer(s, SP - o, SP)
        arrived(st_recv.at[came], st_s.at[o - 1], st_r.at[o - 1], sp=came)
    state = startt[pl.ds(pl.multiple_of(s * vr, vr), vr), :]
    for k in range(SP):
        pre_send[k] = state.astype(BF16)
        if k < SP - 1:
            state = state * jnp.exp(dlog[k][0:1, :]) + st_recv[k].astype(F32)
    pre_recv[s] = pre_send[s]
    for o in range(1, SP):
        to = peer(s, o, SP)
        send(pre_send.at[to], pre_recv.at[s], pre_s.at[o - 1], pre_r.at[o - 1], sp=to)

    third()
    arrived(kv.at[0], kv_s, kv_r, sp=left)
    kvs = jnp.concatenate([kv[0], kv[1]], axis=0)
    kw, vw = kvs[:, :HD], kvs[:, HD:]
    qi = lax.broadcasted_iota(jnp.int32, (TOK, 2 * TOK), 0)
    ki = lax.broadcasted_iota(jnp.int32, (TOK, 2 * TOK), 1)
    distance = qi - ki + TOK
    allowed = (distance >= 0) & (distance < TOK) & ((ki >= TOK) | (s > 0))
    far = distance.astype(F32)
    nears = []
    for h in range(HEADS):
        qh = second[:, C_WQ - C_LQ + h * HD:C_WQ - C_LQ + (h + 1) * HD]
        scores = over(qh, kw, 1, 1) * (HD ** -0.5)
        head = jnp.full((1, 1), t * HEADS + h + 1, jnp.int32).astype(F32)
        slope = jnp.exp2(-8.0 * head / (HEADS * TP))
        weights = jnp.where(allowed, jnp.exp(scores - slope * far), 0.0)
        total = jnp.sum(weights, axis=1, keepdims=True) + jnp.exp(sink_ref[0:1, h:h + 1])
        probs = (weights / total).astype(BF16)
        nears.append(over(probs, vw, 1, 0).astype(BF16))
    og[f, :, :HEADS * HD] = jnp.concatenate(nears, axis=1)

    def share(part_index):
        lanes = pl.ds(part_index * DV, DV)
        for o in range(1, FS):
            send(og.at[f, :, lanes], og.at[f, :, lanes], og_s.at[part_index, o - 1],
                 og_r.at[part_index, o - 1], fs=peer(f, o, FS))

    def shared(part_index):
        lanes = pl.ds(part_index * DV, DV)
        for o in range(1, FS):
            came = peer(f, FS - o, FS)
            arrived(og.at[came, :, lanes], og_s.at[part_index, o - 1],
                    og_r.at[part_index, o - 1], fs=came)

    share(0)
    while done[0] <= half:
        third()
    per = 128 // q
    for k in range(SP // per):
        for side in range(2):
            wcat[side * DV:(side + 1) * DV, k * 128:(k + 1) * 128] = jnp.concatenate(
                [wo[k * per + i][:, side * q:(side + 1) * q] for i in range(per)], axis=1
            )

    for o in range(1, SP):
        came = peer(s, SP - o, SP)
        arrived(pre_recv.at[came], pre_s.at[o - 1], pre_r.at[o - 1], sp=came)
    before = pre_recv[...].reshape(DV, LK).astype(F32)
    raws[0] = raws[0] + over(query[:SPAN], before, 1, 1, HIGH)
    raws[1] = raws[1] + over(query[SPAN:] * jnp.exp(end0), before, 1, 1, HIGH)
    raw = jnp.concatenate(raws, axis=0)
    gated = raw * lax.rsqrt(jnp.mean(raw * raw, axis=1, keepdims=True) + EPS) * lgain_ref[...]
    og[f, :, DV:] = gated.astype(BF16)
    share(1)
    shared(0)
    shared(1)

    heads = og[...].reshape(FS * TOK, 2 * DV)
    po[...] = over(heads, wcat[...], 1, 0).astype(BF16).reshape(FS, TOK, SP * q)
    for o in range(1, TP):
        to = peer(t, o, TP)
        send(po.at[:, pl.ds(pl.multiple_of(to * tr, tr), tr), :], xr_recv.at[o - 1],
             xr_s.at[o - 1], xr_r.at[o - 1], tp=to)
    total = po[:, pl.ds(pl.multiple_of(t * tr, tr), tr), :].astype(F32)
    for o in range(1, TP):
        came = peer(t, TP - o, TP)
        arrived(xr_recv.at[o - 1], xr_s.at[o - 1], xr_r.at[o - 1], tp=came)
        total = total + xr_recv[o - 1].astype(F32)
    fin_send[...] = total.astype(BF16)
    fin_recv[f] = fin_send[f]
    for o in range(1, FS):
        to = peer(f, o, FS)
        send(fin_send.at[to], fin_recv.at[f], fin_s.at[o - 1], fin_r.at[o - 1], fs=to)
    for o in range(1, FS):
        came = peer(f, FS - o, FS)
        arrived(fin_recv.at[came], fin_s.at[o - 1], fin_r.at[o - 1], fs=came)
    for z in range(SP):
        out_ref[:, z * ROWS:(z + 1) * ROWS] = jnp.concatenate(
            [fin_recv[k][:, z * q:(z + 1) * q] for k in range(FS)], axis=1
        )
    for c in pending:
        c.wait_send()


def local(SP, FS, TP, *arrays):
    (activations, input_norm_gain, wq, wk, wv, lq, lk, lv, down, up, bias, extra, start, sink,
     lgain, wow, wol) = arrays
    q, ft, vr, tr = ROWS // FS, FEAT // FS, DV // SP, TOK // TP
    half = SP // 2
    dma = pltpu.SemaphoreType.DMA
    operands = (
        activations, input_norm_gain.reshape(-1, 128), wq, wk.T, wv.T, lq, lk, lv, down.T, up,
        bias.reshape(1, -1), extra.reshape(1, -1), start.reshape(LK, DV), sink.reshape(1, -1),
        lgain.reshape(1, -1), wow, wol,
    )
    vmem = pl.BlockSpec(memory_space=pltpu.VMEM)
    return pl.pallas_call(
        functools.partial(kernel, SP, FS, TP),
        out_shape=jax.ShapeDtypeStruct((tr, SP * ROWS), BF16),
        in_specs=[vmem] * len(operands),
        out_specs=vmem,
        scratch_shapes=[
            pltpu.VMEM((FS, TOK, ft), BF16),
            pltpu.VMEM((FS, TOK, TP * ft), BF16),
            pltpu.VMEM((TP, RANK + 8, TOK), F32),
            pltpu.VMEM((SP * q, C_END), BF16),
            pltpu.VMEM((SP, 256, 2 * q), BF16),
            pltpu.VMEM((2 * DV, SP * q), BF16),
            pltpu.VMEM((FS - 1, TOK, C_END), BF16),
            pltpu.VMEM((FS - 1, TOK, C_END), BF16),
            pltpu.VMEM((2, TOK, 2 * HD), BF16),
            pltpu.VMEM((SP, vr, LK), BF16),
            pltpu.VMEM((SP, vr, LK), BF16),
            pltpu.VMEM((SP, 8, LK), F32),
            pltpu.VMEM((SP, vr, LK), BF16),
            pltpu.VMEM((SP, vr, LK), BF16),
            pltpu.VMEM((DV, LK), F32),
            pltpu.VMEM((FS, TOK, 2 * DV), BF16),
            pltpu.VMEM((FS, TOK, SP * q), BF16),
            pltpu.VMEM((TP - 1, FS, tr, SP * q), BF16),
            pltpu.VMEM((FS, tr, SP * q), BF16),
            pltpu.VMEM((FS, tr, SP * q), BF16),
            dma((3, 2, half)), dma((3, 2, half)),
            dma((FS - 1,)), dma((FS - 1,)),
            dma((TP - 1,)), dma((TP - 1,)),
            dma((TP - 1,)), dma((TP - 1,)),
            dma((SP - 1,)), dma((SP - 1,)),
            dma((2, FS - 1)), dma((2, FS - 1)),
            dma, dma,
            dma((SP - 1,)), dma((SP - 1,)),
            dma((SP - 1,)), dma((SP - 1,)),
            dma((2, FS - 1)), dma((2, FS - 1)),
            dma((TP - 1,)), dma((TP - 1,)),
            dma((FS - 1,)), dma((FS - 1,)),
        ],
        compiler_params=pltpu.CompilerParams(
            collective_id=0, has_side_effects=True, vmem_limit_bytes=60 * 1024 * 1024
        ),
    )(*operands)


def solution(mesh):
    placed = (
        P(("fs", "sp"), "tp"), P(), P("sp", "tp"), P("sp", "tp"), P("sp", "tp"), P("sp", "tp"),
        P("sp", "tp"), P("sp", "tp"), P(), P(None, "tp"), P("tp"), P(("fs", "sp"), "tp"),
        P("tp", None, None), P("tp"), P(), P("tp", "sp"), P("tp", "sp"),
    )
    sizes = (mesh.shape["sp"], mesh.shape["fs"], mesh.shape["tp"])
    return jax.shard_map(
        functools.partial(local, *sizes), mesh=mesh, in_specs=placed,
        out_specs=P(("fs", "sp", "tp"), None), check_vma=False,
    )
```

time: 281 us -> 95.8 us (0.34)
  waiting for transfers between devices: 171 us -> 0 us
  Pallas kernels: 0 us -> 94.1 us
  starting transfers between devices: 32.7 us -> 0 us
  blocking collectives: 30.2 us -> 0 us
  matrix products: 18.9 us -> 0 us
  between operations: 13.9 us -> 0.01 us
  local copies, waits for them, and re-layouts: 8.35 us -> 1.57 us
  other arithmetic: 5.48 us -> 0 us
    all_gather x2 -> x0, waiting for transfers between devices: 126 us -> none  [in_one_piece(): lax.all_gather(both, axis, axis=dim, tiled=True)]
    pallas_call x0 -> x1, Pallas kernels: none -> 94.1 us  [local(): pl.pallas_call(functools.partial(kernel, SP, FS, TP), out_shape=jax.Shape...]
    ppermute x1 -> x0, waiting for transfers between devices: 30.8 us -> none  [passed_along(): lax.ppermute(value, axis, [(source, source + steps) for source in range(l...]
    all_to_all x1 -> x0, blocking collectives: 30.2 us -> none  [summed_on_arrival(): lax.all_to_all(pieces, axis, split_axis=0, concat_axis=0, tiled=True)]
    all_to_all x3 -> x0, starting transfers between devices: 29.4 us -> none  [from_everyone(): lax.all_to_all(jnp.broadcast_to(x[None], (peers, *x.shape)), axis, 0, 0,...]
    dot_general x18 -> x0, matrix products: 18.9 us -> none  [the longest x6 11.7 us: local(): jnp.dot(normed, segment, preferred_element_type=jnp.float32)]
    all_to_all x3 -> x0, waiting for transfers between devices: 13.9 us -> none  [from_everyone(): lax.all_to_all(jnp.broadcast_to(x[None], (peers, *x.shape)), axis, 0, 0,...]
    ppermute x1 -> x0, starting transfers between devices: 3.28 us -> none  [passed_along(): lax.ppermute(value, axis, [(source, source + steps) for source in range(l...]
  transfers between devices with their start and end apart: 6 -> 0, of which waited for: 4 -> 0; matrix products, arithmetic and copies ran while one was open for 8% -> 0% of each run, Pallas kernels for 0% -> 0%
where the time goes in v1:
time: 95.8 us; the launch traced here: 95.7 us
  Pallas kernels  94.1 us (98%)
  local copies, waits for them, and re-layouts  1.57 us (2%)
    pallas_call x1, Pallas kernels, local(): pl.pallas_call(functools.partial(kernel, SP, FS, TP), out_shape=jax.Shape...  94.1 us

profile of v1, /device:TPU:1, one launch (start us, length us, event | category | flops | bytes accessed | tf_op | source)
XLA Modules:
  0.0 95.7 jit_solution(6957114427502674378)
XLA Ops:
  0.0 94.1 %shard_map.163 = bf16[16,4096]{1,0:T(8,128)(2,1)} custom-call(bf16[128,512]{1,0:T(8,128)(2,1)} %x_ref.1, f32[32,128]{1,0:T(8,128)} %bitcast.13, bf16[256,256]{1,0:T(8,128)(2,1)} %wq_ref.1, bf16[64,256]{1,0:T(8,128)(2,1)} %bitcast.11, bf16[64,256]{1,0:T(8,128)(2,1)} %bitcast.12, bf16[256,128]{1,0:T(8,128)(2,1)} %lq_ref.1, bf16[256,128]{1,0:T(8,128)(2,1)} %lk_ref.1, ...), custom_call_target="tpu_custom_call" | custom-call | tf_op jit(solution)/shard_map/pallas_call | solution.py:360
  94.1 1.6 %copy.19 = bf16[16,4096]{1,0:T(8,128)(2,1)} copy(bf16[16,4096]{1,0:T(8,128)(2,1)} %shard_map.163) | data formatting | bytes 262144

commit v2 on v1

v2 whole, which is shorter than its diff:
```python
import functools

import jax
import jax.numpy as jnp
from jax import lax
from jax.experimental import pallas as pl
from jax.experimental.pallas import tpu as pltpu
from jax.sharding import PartitionSpec as P

MESH = pl.DeviceIdType.MESH
HD = 64
HEADS = 4
LK = 128
DV = 256
SPAN = 64
TOK = 128
FEAT = 512
ROWS = 256
RANK = 16
EPS = 1e-05
HIGH = lax.Precision.HIGHEST
F32 = jnp.float32
BF16 = jnp.bfloat16
C_LK, C_LV, C_LQ, C_WQ, C_KV, C_END = 0, 128, 384, 512, 768, 896
RINGS = ((0, 384), (384, 512))
PARTS = ((0, 384), (768, 128), (384, 384))


def over(a, b, ca, cb, precision=None):
    return lax.dot_general(
        a, b, (((ca,), (cb,)), ((), ())), preferred_element_type=F32, precision=precision
    )


def kernel(
    SP, FS, TP,
    x_hbm, gain_hbm, wq_hbm, wkt_hbm, wvt_hbm, lq_hbm, lk_hbm, lv_hbm, ddt_hbm, up_hbm,
    bias_hbm, extra_hbm, start_hbm, sink_hbm, lgain_hbm, wow_hbm, wol_hbm,
    out_hbm,
    out_ref, x_ref, gain_ref, wkt_ref, wvt_ref, ddt_ref, up_ref, bias_ref, extra_ref, start_ref,
    sink_ref, lgain_ref, wow_ref, wol_ref,
    xs, xg, aux, wg, wo, wcat, rs_send, rs_recv, kv, st_send, st_recv, dlog, pre_send,
    pre_recv, startt, og, po, pr_recv, pr_send, xr_recv, fin,
    in_s, out_s, h_s, h_r, w_s, w_r, ring_s, ring_r, y_s, y_r, x_s, x_r, xf_s, xf_r, a_s, a_r, d_s, d_r, rs_s, rs_r, kv_s, kv_r,
    st_s, st_r, pre_s, pre_r, og_s, og_r, pr_s, pr_r, xr_s, xr_r, none_s, none_r,
):
    s, f, t = lax.axis_index("sp"), lax.axis_index("fs"), lax.axis_index("tp")
    q = ROWS // FS
    ft = FEAT // FS
    vr = DV // SP
    tr = TOK // TP
    dim = FEAT * TP
    X = TP // 2
    xi, core = t // 2, lax.rem(t, 2)
    twin = xi * 2 + 1 - core
    right, left = lax.rem(s + 1, SP), lax.rem(s + SP - 1, SP)

    def peer(me, offset, count):
        return lax.rem(me + offset, count)

    def copy(src, dst, send_sem, recv_sem, **device):
        return pltpu.make_async_remote_copy(
            src_ref=src, dst_ref=dst, send_sem=send_sem, recv_sem=recv_sem,
            device_id=device, device_id_type=MESH,
        )

    def send(src, dst, send_sem, recv_sem, **device):
        copy(src, dst, send_sem, recv_sem, **device).start()

    def arrived(ref, recv_sem):
        copy(ref, ref, none_s, recv_sem, tp=twin).wait_recv()

    def left_here(ref, send_sem):
        copy(ref, ref, send_sem, none_r, tp=twin).wait_send()

    barrier = pltpu.get_barrier_semaphore()
    pl.semaphore_signal(barrier, inc=1, device_id={"sp": right}, device_id_type=MESH)
    pl.semaphore_signal(barrier, inc=1, device_id={"sp": left}, device_id_type=MESH)
    for o in range(1, FS):
        pl.semaphore_signal(barrier, inc=1, device_id={"fs": peer(f, o, FS)}, device_id_type=MESH)
    for o in range(1, TP):
        pl.semaphore_signal(barrier, inc=1, device_id={"tp": peer(t, o, TP)}, device_id_type=MESH)

    mine = pl.ds(pl.multiple_of(s * q, q), q)
    part = pl.ds(pl.multiple_of(f * q, q), q)
    loads = []
    for src, dst in (
        (lk_hbm.at[part, :], wg.at[core, mine, pl.ds(C_LK, LK)]),
        (lv_hbm.at[part, :], wg.at[core, mine, pl.ds(C_LV, DV)]),
        (lq_hbm.at[part, :], wg.at[core, mine, pl.ds(C_LQ, LK)]),
        (wq_hbm.at[part, :], wg.at[core, mine, pl.ds(C_WQ, HEADS * HD)]),
        (wkt_hbm, wkt_ref), (wvt_hbm, wvt_ref), (x_hbm, x_ref), (gain_hbm, gain_ref),
        (ddt_hbm, ddt_ref), (wow_hbm, wow_ref), (wol_hbm, wol_ref), (start_hbm, start_ref),
        (up_hbm, up_ref), (bias_hbm, bias_ref), (extra_hbm, extra_ref), (sink_hbm, sink_ref),
        (lgain_hbm, lgain_ref),
    ):
        c = pltpu.make_async_copy(src, dst, in_s.at[len(loads)])
        c.start()
        loads.append(c)
    for c in loads[:6]:
        c.wait()
    both = jnp.concatenate([wkt_ref[...], wvt_ref[...]], axis=0).astype(F32).T.astype(BF16)
    for k in range(FS):
        @pl.when(f == k)
        def _():
            wg[core, mine, C_KV:C_END] = both[k * q:(k + 1) * q, :]

    pl.semaphore_wait(barrier, 2 + (FS - 1) + (TP - 1))

    half = SP // 2

    both_cores = pl.ds(0, 2)

    def chunk(stream, z, cores):
        if stream >= 4:
            return wo.at[cores, z, pl.ds(stream % 2 * LK, LK)]
        at, width = RINGS[stream // 2]
        h = q // 2
        rows = pl.ds(pl.multiple_of(z * q + stream % 2 * h, h), h)
        return wg.at[cores, rows, pl.ds(at, width)]

    groups = (0, 0, 1, 1, 2, 3)

    def carrier(group):
        return (1, 0, 1, 0)[group]

    def carries(group):
        return core == carrier(group)

    def own_copy(group):
        guest = 1 - carrier(group)
        if group >= 2:
            src = wo.at[guest, s, pl.ds((group - 2) * LK, LK)]
        else:
            at, width = RINGS[group]
            src = wg.at[guest, mine, pl.ds(at, width)]
        return copy(src, src, h_s.at[group], h_r.at[group], tp=twin)

    counts = (half, SP - 1 - half)

    def ring_copy(stream, d, k):
        z = lax.rem(s + SP - k, SP) if d == 0 else lax.rem(s + k, SP)
        ref = chunk(stream, z, both_cores)
        return copy(ref, ref, ring_s.at[groups[stream]], ring_r.at[stream, d, k],
                    sp=right if d == 0 else left)

    def from_ring(stream, d, k):
        arrived(chunk(stream, 0, both_cores), ring_r.at[stream, d, k])

    def twin_copy(stream, d, k):
        z = lax.rem(s + SP - 1 - k, SP) if d == 0 else lax.rem(s + k + 1, SP)
        ref = chunk(stream, z, 1 - carrier(groups[stream]))
        return copy(ref, ref, w_s.at[groups[stream]], w_r.at[groups[stream]], tp=twin)

    def ring_step(stream, k):
        @pl.when(carries(groups[stream]))
        def _():
            if k == 0 and (stream % 2 == 0 or stream > 3):
                own_copy(groups[stream]).wait_recv()
            for d in range(2):
                if 1 <= k <= counts[d]:
                    from_ring(stream, d, k - 1)
                if k < counts[d]:
                    ring_copy(stream, d, k).start()
                if 1 <= k <= counts[d]:
                    twin_copy(stream, d, k - 1).start()

    def many(group, cores):
        if group >= 2:
            return wo.at[cores, pl.ds(0, SP - 1), pl.ds((group - 2) * LK, LK)]
        at, width = RINGS[group]
        return wg.at[cores, pl.ds(0, (SP - 1) * q), pl.ds(at, width)]

    def landed(group):
        @pl.when(jnp.logical_not(carries(group)))
        def _():
            arrived(many(group, 1 - carrier(group)), w_r.at[group])

    done = [0]

    def lagging():
        if done[0] <= half:
            ring_step(4, done[0])
            ring_step(5, done[0])
            done[0] += 1

    def second_group(k):
        ring_step(2, k)
        ring_step(3, k)

    def tick(k):
        ring_step(0, k)
        ring_step(1, k)
        if k < half - 1:
            second_group(k)
        if k >= 2 and k % 2 == 0:
            lagging()

    @pl.when(core == 0)
    def _():
        own_copy(0).start()

    @pl.when(core == 1)
    def _():
        own_copy(1).start()

    tick(0)

    for c in loads[6:11]:
        c.wait()
    for k in range(FS):
        @pl.when(f == k)
        def _():
            wo[core, s] = jnp.concatenate(
                [wow_ref[:, k * q:(k + 1) * q], wol_ref[:, k * q:(k + 1) * q]], axis=1
            )
    xf = x_ref[...].astype(F32)
    @pl.when(core == 0)
    def _():
        own_copy(2).start()

    @pl.when(core == 1)
    def _():
        own_copy(3).start()

    rows = FEAT // 128
    gain = jnp.concatenate(
        [gain_ref[pl.ds(t * rows + k, 1), :] for k in range(rows)], axis=1
    )
    xw = (xf * gain).astype(BF16)
    here = pl.ds(pl.multiple_of(t * ft, ft), ft)
    for k in range(FS):
        cut = jnp.concatenate(
            [xw[:, k * q:(k + 1) * q], xw[:, ROWS + k * q:ROWS + (k + 1) * q]], axis=1
        )
        xs[k] = cut

        @pl.when(f == k)
        def _():
            xg[k, :, here] = cut
    for o in range(1, FS):
        to = peer(f, o, FS)
        send(xs.at[to], xg.at[f, :, here], y_s, y_r, fs=to)
    dd = ddt_ref[:, pl.ds(pl.multiple_of(t * FEAT, FEAT), FEAT)]
    aux[t, :RANK, :] = over(dd, xw, 1, 1)
    aux[t, RANK:, :] = over(jnp.ones((8, FEAT), F32), xf * xf, 1, 1, HIGH)
    for o in range(1, TP):
        send(aux.at[t], aux.at[t], a_s, a_r, tp=peer(t, o, TP))

    tick(1)
    arrived(xg.at[pl.ds(0, FS - 1), :, here], y_r)
    for o in range(1, X):
        send(xg.at[:, :, here], xg.at[:, :, here], x_s, x_r.at[o - 1],
             tp=peer(xi, o, X) * 2 + core)
    send(xg.at[:, :, here], xg.at[:, :, here], x_s, x_r.at[X - 1], tp=twin)
    for c in loads[11:]:
        c.wait()
    startt[...] = start_ref[...].T
    early = max(2, 3 * half // 4)
    for k in range(2, early):
        tick(k)

    def lanes_of(device):
        return pl.ds(pl.multiple_of(device * ft, ft), ft)

    for o in range(1, X):
        came = peer(xi, X - o, X) * 2 + core
        chunk_x = xg.at[:, :, lanes_of(came)]
        arrived(chunk_x, x_r.at[o - 1])
        send(chunk_x, chunk_x, xf_s, xf_r, tp=twin)
    tick(early)
    arrived(aux.at[pl.ds(0, TP - 1)], a_r)
    sums = aux[0]
    for k in range(1, TP):
        sums = sums + aux[k]
    scale_rows = lax.rsqrt(sums[RANK:, :] / dim + EPS)
    eighth = jnp.full((8, 128), 0.125, F32)
    scale = over(scale_rows, eighth, 0, 0, HIGH)
    low = (sums[:RANK, :] * scale_rows[0:1, :]).astype(BF16)
    energies = over(low, up_ref[...], 0, 0) + bias_ref[...]
    extra = over(jnp.broadcast_to(extra_ref[...], (8, 128)), eighth, 0, 0, HIGH)
    fading = (
        jnp.minimum(energies, 0.0) - jnp.log1p(jnp.exp(-jnp.abs(energies)))
    ) / 16.0 + extra
    ri = lax.broadcasted_iota(jnp.int32, (TOK, TOK), 0)
    ci = lax.broadcasted_iota(jnp.int32, (TOK, TOK), 1)
    tri = ((ri >= ci) & ((ri < SPAN) | (ci >= SPAN))).astype(F32)
    running = over(tri, fading, 1, 0, HIGH)
    end0, end1 = running[SPAN - 1:SPAN, :], running[TOK - 1:TOK, :]
    dlog[s] = jnp.broadcast_to(end0 + end1, (8, 128))
    for k in range(early + 1, half + 1):
        tick(k)
    landed(0)
    arrived(xg.at[:, :, lanes_of(twin)], x_r.at[X - 1])
    if X > 1:
        arrived(xg.at[:, :, pl.ds(0, (X - 1) * ft)], xf_r)

    owns = []

    def project(part_index):
        at, width = PARTS[part_index]
        cols = pl.ds(at, width)
        for o in list(range(1, FS)) + [0]:
            to = peer(f, o, FS)
            product = over(xg[to], wg[core, :, at:at + width], 1, 0)
            if o == 0:
                owns.append(product)
            else:
                rs_send[o - 1, :, at:at + width] = product.astype(BF16)
                send(rs_send.at[o - 1, :, cols], rs_recv.at[o - 1, :, cols],
                     rs_s, rs_r.at[part_index], fs=to)

    def reduced(part_index):
        at, width = PARTS[part_index]
        total = owns[part_index]
        arrived(rs_recv.at[:, :, pl.ds(at, width)], rs_r.at[part_index])
        for o in range(1, FS):
            total = total + rs_recv[o - 1, :, at:at + width].astype(F32)
        wide = jnp.concatenate([scale] * (width // 128), axis=1)
        return (total * wide).astype(BF16)

    project(0)
    for o in range(1, SP):
        send(dlog.at[s], dlog.at[s], d_s, d_r, sp=peer(s, o, SP))
    second_group(half - 1)
    lagging()
    second_group(half)
    first = reduced(0)
    keys = first[:, C_LK:C_LV].astype(F32)
    values = first[:, C_LV:C_LQ].astype(F32)
    grow = jnp.exp(running)
    ends = jnp.where(ri < SPAN, end0, end1)
    ending = keys * jnp.exp(ends - running)
    state0 = over(values[:SPAN], ending[:SPAN], 0, 0, HIGH)
    state1 = state0 * jnp.exp(end1) + over(values[SPAN:], ending[SPAN:], 0, 0, HIGH)
    packed = state1.astype(BF16)
    st_send[...] = packed.reshape(SP, vr, LK)
    st_recv[s] = st_send[s]
    for o in range(1, SP):
        to = peer(s, o, SP)
        send(st_send.at[to], st_recv.at[s], st_s, st_r, sp=to)

    lagging()
    landed(1)
    project(1)
    project(2)
    lagging()
    arrived(dlog.at[pl.ds(0, SP - 1)], d_r)
    arrived(st_recv.at[pl.ds(0, SP - 1)], st_r)
    state = startt[pl.ds(pl.multiple_of(s * vr, vr), vr), :]
    for k in range(SP):
        pre_send[k] = state.astype(BF16)
        if k < SP - 1:
            state = state * jnp.exp(dlog[k][0:1, :]) + st_recv[k].astype(F32)
    pre_recv[s] = pre_send[s]
    for o in range(1, SP):
        to = peer(s, o, SP)
        send(pre_send.at[to], pre_recv.at[s], pre_s, pre_r, sp=to)
    lagging()
    kv[1] = reduced(1)
    send(kv.at[1], kv.at[0], kv_s, kv_r, sp=right)
    lagging()
    second = reduced(2)
    lagging()
    inverse = keys * jnp.exp(-running)
    query = second[:, :C_WQ - C_LQ].astype(F32) * (LK ** -0.5) * grow
    raws = []
    for n in range(2):
        span = slice(n * SPAN, (n + 1) * SPAN)
        inner = over(query[span], inverse[span], 1, 1, HIGH)
        inner = jnp.where(ri[:SPAN, :SPAN] >= ci[:SPAN, :SPAN], inner, 0.0)
        raws.append(over(inner, values[span], 1, 0, HIGH))
    raws[1] = raws[1] + over(query[SPAN:], state0, 1, 1, HIGH)
    arrived(kv.at[0], kv_r)
    kvs = jnp.concatenate([kv[0], kv[1]], axis=0)
    kw, vw = kvs[:, :HD], kvs[:, HD:]
    qi = lax.broadcasted_iota(jnp.int32, (TOK, 2 * TOK), 0)
    ki = lax.broadcasted_iota(jnp.int32, (TOK, 2 * TOK), 1)
    distance = qi - ki + TOK
    allowed = (distance >= 0) & (distance < TOK) & ((ki >= TOK) | (s > 0))
    far = distance.astype(F32)
    nears = []
    for h in range(HEADS):
        qh = second[:, C_WQ - C_LQ + h * HD:C_WQ - C_LQ + (h + 1) * HD]
        scores = over(qh, kw, 1, 1) * (HD ** -0.5)
        head = jnp.full((1, 1), t * HEADS + h + 1, jnp.int32).astype(F32)
        slope = jnp.exp2(-8.0 * head / (HEADS * TP))
        weights = jnp.where(allowed, jnp.exp(scores - slope * far), 0.0)
        total = jnp.sum(weights, axis=1, keepdims=True) + jnp.exp(sink_ref[0:1, h:h + 1])
        probs = (weights / total).astype(BF16)
        nears.append(over(probs, vw, 1, 0).astype(BF16))
    og[f, :, :HEADS * HD] = jnp.concatenate(nears, axis=1)

    def share(part_index):
        lanes = pl.ds(part_index * DV, DV)
        for o in range(1, FS):
            send(og.at[f, :, lanes], og.at[f, :, lanes], og_s, og_r.at[part_index, o - 1],
                 fs=peer(f, o, FS))

    share(0)
    while done[0] <= half:
        lagging()
    landed(2)
    landed(3)
    per = 128 // q
    for k in range(SP // per):
        for side in range(2):
            wcat[side * DV:(side + 1) * DV, k * 128:(k + 1) * 128] = jnp.concatenate(
                [wo[core, k * per + i][:, side * q:(side + 1) * q] for i in range(per)], axis=1
            )

    arrived(pre_recv.at[pl.ds(0, SP - 1)], pre_r)
    before = pre_recv[...].reshape(DV, LK).astype(F32)
    raws[0] = raws[0] + over(query[:SPAN], before, 1, 1, HIGH)
    raws[1] = raws[1] + over(query[SPAN:] * jnp.exp(end0), before, 1, 1, HIGH)
    raw = jnp.concatenate(raws, axis=0)
    gated = raw * lax.rsqrt(jnp.mean(raw * raw, axis=1, keepdims=True) + EPS) * lgain_ref[...]
    og[f, :, DV:] = gated.astype(BF16)
    share(1)
    order = [0] + sorted(range(1, FS), key=lambda o: min(o, FS - o))

    def chip_sum(o):
        arrived(pr_recv.at[o], pr_r.at[o])
        for e in range(X):
            to = peer(xi, e, X)
            both = po[o, to, core].astype(F32) + pr_recv[o, to].astype(F32)
            pr_send[o, e] = both.astype(BF16)
            if o > 0 or e > 0:
                send(pr_send.at[o, e], xr_recv.at[o, e], xr_s.at[min(o, 1)], xr_r.at[o],
                     tp=to * 2 + core, fs=peer(f, o, FS))

    for i, o in enumerate(order):
        source = peer(f, o, FS)
        if o > 0:
            for part_index in range(2):
                arrived(og.at[source, :, pl.ds(part_index * DV, DV)],
                        og_r.at[part_index, FS - 1 - o])
        po[o] = over(og[source], wcat[...], 1, 0).astype(BF16).reshape(X, 2, tr, SP * q)
        send(po.at[o, :, 1 - core], pr_recv.at[o], pr_s, pr_r.at[o], tp=twin)
        if i > 0:
            chip_sum(order[i - 1])
    chip_sum(order[-1])
    for o in order:
        if o > 0:
            arrived(xr_recv.at[o], xr_r.at[o])
            total = xr_recv[o, 0].astype(F32)
        else:
            if X > 1:
                arrived(xr_recv.at[o, pl.ds(1, X - 1)], xr_r.at[o])
            total = pr_send[o, 0].astype(F32)
        for e in range(1, X):
            total = total + xr_recv[o, e].astype(F32)
        fin[peer(f, FS - o, FS)] = total.astype(BF16)
    stored = []
    for side in range(2):
        for z in range(side * half, (side + 1) * half):
            out_ref[:, z * ROWS:(z + 1) * ROWS] = jnp.concatenate(
                [fin[k][:, z * q:(z + 1) * q] for k in range(FS)], axis=1
            )
        lanes = pl.ds(side * half * ROWS, half * ROWS)
        c = pltpu.make_async_copy(out_ref.at[:, lanes], out_hbm.at[:, lanes], out_s.at[side])
        c.start()
        stored.append(c)
    for group in range(4):
        @pl.when(carries(group))
        def _():
            left_here(many(group, both_cores), ring_s.at[group])
            left_here(many(group, 1 - carrier(group)), w_s.at[group])

        @pl.when(jnp.logical_not(carries(group)))
        def _():
            own_copy(group).wait_send()

    left_here(xs.at[pl.ds(0, FS - 1)], y_s)
    left_here(xg.at[:, :, pl.ds(0, X * ft)], x_s)
    if X > 1:
        left_here(xg.at[:, :, pl.ds(0, (X - 1) * ft)], xf_s)
        left_here(pr_send.at[0, pl.ds(1, X - 1)], xr_s.at[0])
    left_here(aux.at[pl.ds(0, TP - 1)], a_s)
    left_here(dlog.at[pl.ds(0, SP - 1)], d_s)
    left_here(rs_send, rs_s)
    left_here(kv.at[0], kv_s)
    left_here(st_send.at[pl.ds(0, SP - 1)], st_s)
    left_here(pre_send.at[pl.ds(0, SP - 1)], pre_s)
    left_here(og.at[pl.ds(0, FS - 1)], og_s)
    left_here(po.at[:, :, 0], pr_s)
    left_here(pr_send.at[pl.ds(1, FS - 1)], xr_s.at[1])
    for c in stored:
        c.wait()


def local(SP, FS, TP, *arrays):
    (activations, input_norm_gain, wq, wk, wv, lq, lk, lv, down, up, bias, extra, start, sink,
     lgain, wow, wol) = arrays
    q, ft, vr, tr = ROWS // FS, FEAT // FS, DV // SP, TOK // TP
    half = SP // 2
    dma = pltpu.SemaphoreType.DMA
    operands = (
        activations, input_norm_gain.reshape(-1, 128), wq, wk.T, wv.T, lq, lk, lv, down.T, up,
        bias.reshape(1, -1), extra.reshape(1, -1), start.reshape(LK, DV), sink.reshape(1, -1),
        lgain.reshape(1, -1), wow, wol,
    )
    held = [operands[i] for i in (0, 1, 3, 4, 8, 9, 10, 11, 12, 13, 14, 15, 16)]
    X = TP // 2
    return pl.pallas_call(
        functools.partial(kernel, SP, FS, TP),
        out_shape=jax.ShapeDtypeStruct((tr, SP * ROWS), BF16),
        in_specs=[pl.BlockSpec(memory_space=pl.ANY)] * len(operands),
        out_specs=pl.BlockSpec(memory_space=pl.ANY),
        scratch_shapes=[pltpu.VMEM((tr, SP * ROWS), BF16)] + [pltpu.VMEM(a.shape, a.dtype) for a in held] + [
            pltpu.VMEM((FS, TOK, ft), BF16),
            pltpu.VMEM((FS, TOK, TP * ft), BF16),
            pltpu.VMEM((TP, RANK + 8, TOK), F32),
            pltpu.VMEM((2, SP * q, C_END), BF16),
            pltpu.VMEM((2, SP, 256, 2 * q), BF16),
            pltpu.VMEM((2 * DV, SP * q), BF16),
            pltpu.VMEM((FS - 1, TOK, C_END), BF16),
            pltpu.VMEM((FS - 1, TOK, C_END), BF16),
            pltpu.VMEM((2, TOK, 2 * HD), BF16),
            pltpu.VMEM((SP, vr, LK), BF16),
            pltpu.VMEM((SP, vr, LK), BF16),
            pltpu.VMEM((SP, 8, LK), F32),
            pltpu.VMEM((SP, vr, LK), BF16),
            pltpu.VMEM((SP, vr, LK), BF16),
            pltpu.VMEM((DV, LK), F32),
            pltpu.VMEM((FS, TOK, 2 * DV), BF16),
            pltpu.VMEM((FS, X, 2, tr, SP * q), BF16),
            pltpu.VMEM((FS, X, tr, SP * q), BF16),
            pltpu.VMEM((FS, X, tr, SP * q), BF16),
            pltpu.VMEM((FS, X, tr, SP * q), BF16),
            pltpu.VMEM((FS, tr, SP * q), BF16),
            dma((len(operands),)), dma((2,)),
            dma((4,)), dma((4,)),
            dma((4,)), dma((4,)),
            dma((4,)), dma((6, 2, half)),
            dma, dma,
            dma, dma((X,)),
            dma, dma,
            dma, dma,
            dma, dma,
            dma, dma((3,)),
            dma, dma,
            dma, dma,
            dma, dma,
            dma, dma((2, FS - 1)),
            dma, dma((FS,)),
            dma((2,)), dma((FS,)),
            dma, dma,
        ],
        compiler_params=pltpu.CompilerParams(
            collective_id=0, has_side_effects=True, vmem_limit_bytes=60 * 1024 * 1024
        ),
    )(*operands)


def solution(mesh):
    placed = (
        P(("fs", "sp"), "tp"), P(), P("sp", "tp"), P("sp", "tp"), P("sp", "tp"), P("sp", "tp"),
        P("sp", "tp"), P("sp", "tp"), P(), P(None, "tp"), P("tp"), P(("fs", "sp"), "tp"),
        P("tp", None, None), P("tp"), P(), P("tp", "sp"), P("tp", "sp"),
    )
    sizes = (mesh.shape["sp"], mesh.shape["fs"], mesh.shape["tp"])
    return jax.shard_map(
        functools.partial(local, *sizes), mesh=mesh, in_specs=placed,
        out_specs=P(("fs", "sp", "tp"), None), check_vma=False,
    )
```

time: 95.8 us -> 89.4 us (0.933)
  Pallas kernels: 94.1 us -> 87.6 us
    pallas_call x1, Pallas kernels: 94.1 us -> 87.6 us  [local(): pl.pallas_call(functools.partial(kernel, SP, FS, TP), out_shape=jax.Shape...]
where the time goes in v2:
time: 89.4 us; the launch traced here: 89.2 us
  Pallas kernels  87.6 us (98%)
  local copies, waits for them, and re-layouts  1.57 us (2%)
    pallas_call x1, Pallas kernels, local(): pl.pallas_call(functools.partial(kernel, SP, FS, TP), out_shape=jax.Shape...  87.6 us

profile of v2, /device:TPU:1, one launch (start us, length us, event | category | flops | bytes accessed | tf_op | source)
XLA Modules:
  0.0 89.2 jit_solution(2470305929452376619)
XLA Ops:
  0.0 87.6 %shard_map.163 = bf16[16,4096]{1,0:T(8,128)(2,1)} custom-call(bf16[128,512]{1,0:T(8,128)(2,1)} %x_hbm.1, f32[32,128]{1,0:T(8,128)} %bitcast.13, bf16[256,256]{1,0:T(8,128)(2,1)} %wq_hbm.1, bf16[64,256]{1,0:T(8,128)(2,1)} %bitcast.11, bf16[64,256]{1,0:T(8,128)(2,1)} %bitcast.12, bf16[256,128]{1,0:T(8,128)(2,1)} %lq_hbm.1, bf16[256,128]{1,0:T(8,128)(2,1)} %lk_hbm.1, ...), custom_call_target="tpu_custom_call" | custom-call | tf_op jit(solution)/shard_map/pallas_call | solution.py:505
  87.6 1.6 %copy.19 = bf16[16,4096]{1,0:T(8,128)(2,1)} copy(bf16[16,4096]{1,0:T(8,128)(2,1)} %shard_map.163) | data formatting | bytes 262144
